TPU v7x, 32 devices: a whole 2x2x4 slice. The times are simulated.
32 devices in a mesh: kv: 8 (over z, y), tp: 4 (over x, core).
Axes of the slice: x: 2, y: 2, z: 4, core: 2. Of those that a mesh axis runs over, the one named last changes fastest.
Arguments:
- tokens: bfloat16 [1024, 4096], P(None, 'kv'), may hold values from -6 to 6
- norm_gain: float32 [4096], replicated, may hold values from 0.1 to 1.9
- query_weight: bfloat16 [4096, 2048], P('kv', 'tp'), may hold values from -0.09375 to 0.09375
- key_weight: bfloat16 [4096, 2048], P('kv', 'tp'), may hold values from -0.09375 to 0.09375
- value_weight: bfloat16 [4096, 4096], P('kv', 'tp'), may hold values from -0.09375 to 0.09375
- outgate_weight: bfloat16 [4096, 4096], P('kv', 'tp'), may hold values from -0.09375 to 0.09375
- gate_weight: bfloat16 [4096, 32], P('kv'), may hold values from -0.09375 to 0.09375
- forget_bias: float32 [16], replicated, may hold values from -1 to 5
- head_gain: float32 [4096], P('tp'), may hold values from 0.1 to 1.9
- output_weight: bfloat16 [4096, 4096], P('tp', 'kv'), may hold values from -0.09375 to 0.09375
- state_matrix: float32 [256, 16, 128, 256], P('kv', 'tp'), may hold values from -6 to 6
- state_normal: float32 [256, 16, 128], P('kv', 'tp'), may hold values from -6 to 6
- state_stable: float32 [256, 16], P('kv', 'tp'), may hold values from -3 to 3
- prior_keys: bfloat16 [256, 4, 2048], P('kv', None, 'tp'), may hold values from -0.59765625 to 0.59765625
- prior_values: bfloat16 [256, 4, 4096], P('kv', None, 'tp'), may hold values from -6 to 6
- prior_ingate: float32 [256, 4, 16], P('kv', None, 'tp'), may hold values from -4 to 4
- prior_forget: float32 [256, 4, 16], P('kv', None, 'tp'), may hold values from -2 to -0.02
- accepted: int32 [256], P('kv'), may hold values from 0 to 4
- parents: int32 [256, 4], P('kv'), may hold values from -1 to 2, as said below
Outputs:
- layer_out: bfloat16 [1024, 4096], P('tp', 'kv')
- new_matrix: float32 [256, 16, 128, 256], P('kv', 'tp')
- new_normal: float32 [256, 16, 128], P('kv', 'tp')
- new_stable: float32 [256, 16], P('kv', 'tp')
Inputs may be any that keep to these rules, and one draw needn't show every extreme that they name: parents of proposal t lie in -1 to t - 1; the first proposal's parent is -1; in some sequence each proposal's parent is the one before it.
All inputs are finite; a program needn't handle non-finite values.
Results may differ from a plain program's by a relative error of at most 0.0089.
Values may be sent and summed in bfloat16 or wider, within the bound.
No kernel may reach another device: no remote copies, remote signals or barrier semaphores. Data moves between devices by JAX's collectives and lax.ppermute only.
A program may use at most 128 MiB of HBM per device.

v0:
```python
import jax
import jax.numpy as jnp
from jax import lax
from jax.sharding import PartitionSpec as P

D = 4096
HEADS = 16
DQK = 128
DV = 256
PROP = 4


def ancestry(parents):
    count = parents.shape[1]
    index = jnp.arange(count, dtype=jnp.int32)
    current = jnp.broadcast_to(index[None, :], parents.shape)
    table = jnp.broadcast_to(
        (index[:, None] == index[None, :]).astype(jnp.float32), (parents.shape[0], count, count)
    )
    for repeat in range(count - 1):
        looked = jnp.take_along_axis(parents, jnp.maximum(current, 0), axis=1)
        current = jnp.where(current >= 0, looked, -1)
        table = table + (current[:, :, None] == index[None, None, :]).astype(jnp.float32)
    return table


def commit(matrix, normal, stable, prior_k, prior_v, prior_i, prior_f, accepted):
    count = prior_k.shape[1]
    live = (jnp.arange(count, dtype=jnp.int32)[None, :] < accepted[:, None])[:, :, None]
    forget_live = jnp.where(live, prior_f, 0.0)
    cumul = jnp.cumsum(forget_live, axis=1)
    total = cumul[:, -1]
    weight_log = jnp.where(live, total[:, None, :] - cumul + prior_i, -jnp.inf)
    new_stable = jnp.maximum(total + stable, jnp.max(weight_log, axis=1))
    weights = jnp.exp(weight_log - new_stable[:, None, :])
    decay = jnp.exp(total + stable - new_stable)
    hp = lax.Precision.HIGHEST
    new_matrix = decay[:, :, None, None] * matrix + jnp.einsum(
        "sph,sphd,sphv->shdv", weights, prior_k, prior_v, precision=hp
    )
    new_normal = decay[:, :, None] * normal + jnp.einsum(
        "sph,sphd->shd", weights, prior_k, precision=hp
    )
    return (new_matrix, new_normal, new_stable)


def tree_read(query, key_rows, value_rows, ingate, logforget, table, matrix, normal, stable):
    hp = lax.Precision.HIGHEST
    path_sum = jnp.einsum("sta,sah->sth", table, logforget, precision=hp)
    dlog = path_sum[:, :, None, :] - path_sum[:, None, :, :] + ingate[:, None, :, :]
    dlog = jnp.where(table[:, :, :, None] > 0.5, dlog, -jnp.inf)
    carried = path_sum + stable[:, None, :]
    top = jnp.maximum(carried, jnp.max(dlog, axis=2))
    scores = jnp.einsum("sthd,sahd->stah", query, key_rows, precision=hp) * jnp.exp(
        dlog - top[:, :, None, :]
    )
    factor = jnp.exp(carried - top)
    numer = jnp.einsum("stah,sahv->sthv", scores, value_rows, precision=hp) + factor[
        ..., None
    ] * jnp.einsum("sthd,shdv->sthv", query, matrix, precision=hp)
    denom = jnp.sum(scores, axis=2) + factor * jnp.einsum(
        "sthd,shd->sth", query, normal, precision=hp
    )
    return numer / jnp.maximum(jnp.abs(denom), jnp.exp(-top))[..., None]


def head_gate_columns(gate_block, head_start, head_local):
    rows = gate_block.shape[0]
    picked = lax.dynamic_slice_in_dim(gate_block.reshape(rows, 2, HEADS), head_start, head_local, 2)
    return picked.reshape(rows, 2 * head_local)


def per_device(
    tokens,
    norm_gain,
    query_weight,
    key_weight,
    value_weight,
    outgate_weight,
    gate_weight,
    forget_bias,
    head_gain,
    output_weight,
    state_matrix,
    state_normal,
    state_stable,
    prior_keys,
    prior_values,
    prior_ingate,
    prior_forget,
    accepted,
    parents,
):
    f32 = jnp.float32
    head_local = query_weight.shape[1] // DQK
    width_local = tokens.shape[1]
    seq_local = accepted.shape[0]
    row_local = seq_local * PROP
    head_start = lax.axis_index("tp") * head_local
    xfloat = tokens.astype(f32)
    part_squares = jnp.sum(xfloat * xfloat, axis=-1)
    own_gain = lax.dynamic_slice_in_dim(
        norm_gain, lax.axis_index("kv") * width_local, width_local, 0
    )
    normed = (xfloat * own_gain).astype(jnp.bfloat16)
    gate_cols = head_gate_columns(gate_weight, head_start, head_local)
    part_query = jnp.dot(normed, query_weight, preferred_element_type=f32)
    part_key = jnp.dot(normed, key_weight, preferred_element_type=f32)
    part_value = jnp.dot(normed, value_weight, preferred_element_type=f32)
    part_outgate = jnp.dot(normed, outgate_weight, preferred_element_type=f32)
    part_gates = jnp.dot(normed, gate_cols, preferred_element_type=f32)
    all_squares = lax.psum(part_squares, "kv")
    query, key_rows, value_rows, outgate, gates = (
        lax.psum_scatter(part_query, "kv", scatter_dimension=0, tiled=True),
        lax.psum_scatter(part_key, "kv", scatter_dimension=0, tiled=True),
        lax.psum_scatter(part_value, "kv", scatter_dimension=0, tiled=True),
        lax.psum_scatter(part_outgate, "kv", scatter_dimension=0, tiled=True),
        lax.psum_scatter(part_gates, "kv", scatter_dimension=0, tiled=True),
    )
    squares = lax.dynamic_slice_in_dim(all_squares, lax.axis_index("kv") * row_local, row_local, 0)
    scale = lax.rsqrt(squares / D + 1e-06)[:, None]
    query = (scale * query).reshape(seq_local, PROP, head_local, DQK)
    key_rows = (scale * key_rows / jnp.sqrt(jnp.float32(DQK))).reshape(
        seq_local, PROP, head_local, DQK
    )
    value_rows = (scale * value_rows).reshape(seq_local, PROP, head_local, DV)
    outgate = (scale * outgate).reshape(seq_local, PROP, head_local, DV)
    gates = scale * gates
    own_bias = lax.dynamic_slice_in_dim(forget_bias, head_start, head_local, 0)
    ingate = gates[:, :head_local].reshape(seq_local, PROP, head_local)
    logforget = jax.nn.log_sigmoid(gates[:, head_local:] + own_bias).reshape(
        seq_local, PROP, head_local
    )
    new_matrix, new_normal, new_stable = commit(
        state_matrix,
        state_normal,
        state_stable,
        prior_keys.astype(f32).reshape(seq_local, PROP, head_local, DQK),
        prior_values.astype(f32).reshape(seq_local, PROP, head_local, DV),
        prior_ingate,
        prior_forget,
        accepted,
    )
    table = ancestry(parents)
    read = tree_read(
        query, key_rows, value_rows, ingate, logforget, table, new_matrix, new_normal, new_stable
    )
    normer = lax.rsqrt(jnp.mean(read * read, axis=-1, keepdims=True) + 1e-06)
    hidden = read * normer * head_gain.reshape(head_local, DV) * jax.nn.sigmoid(outgate)
    hidden = hidden.reshape(row_local, head_local * DV).astype(jnp.bfloat16)
    partial_out = jnp.dot(
        lax.all_gather(hidden, "kv", axis=0, tiled=True), output_weight, preferred_element_type=f32
    )
    layer_out = lax.psum_scatter(partial_out, "tp", scatter_dimension=0, tiled=True).astype(
        jnp.bfloat16
    )
    return (layer_out, new_matrix, new_normal, new_stable)


def solution(mesh):
    placed = (
        P(None, "kv"),
        P(),
        P("kv", "tp"),
        P("kv", "tp"),
        P("kv", "tp"),
        P("kv", "tp"),
        P("kv", None),
        P(),
        P("tp"),
        P("tp", "kv"),
        P("kv", "tp", None, None),
        P("kv", "tp", None),
        P("kv", "tp"),
        P("kv", None, "tp"),
        P("kv", None, "tp"),
        P("kv", None, "tp"),
        P("kv", None, "tp"),
        P("kv"),
        P("kv", None),
    )
    return jax.shard_map(
        per_device,
        mesh=mesh,
        in_specs=placed,
        out_specs=(P("tp", "kv"), P("kv", "tp", None, None), P("kv", "tp", None), P("kv", "tp")),
        check_vma=False,
    )
```

profile of v0, /device:TPU:0, one launch (start us, length us, event | category | flops | bytes accessed | tf_op | source)
XLA Modules:
  0.0 501.6 jit_solution(12649565121238626551)
XLA Ops:
  7.2 0.8 constant_dynamic-slice_fusion
  8.1 0.8 dynamic_slice.13
  8.8 2.2 fusion.8
  11.1 3.5 fusion.12
  14.8 2.1 fusion.10
  16.9 3.2 fusion.6
  20.2 4.5 fusion.14
  24.8 0.5 copy-done.13
  25.9 1.5 gather_fusion
  27.9 1.5 gather_fusion.1
  29.9 1.5 gather_fusion.2
  32.6 23.3 %psum.7 = f32[1024]{0:T(1024)S(1)} all-reduce(f32[1024]{0:T(1024)S(1)} %fusion), channel_id=1, replica_groups=mesh['kv'=8,'tp'=4] {'kv'}, use_global_device_ids=true, to_apply=%region_1.0 | all-reduce | flops 1024 | bytes 8192 | tf_op jit(solution)/shard_map/psum | solution.py:112
  56.0 13.2 %reduce-scatter.13.cloned.1.call-done = f32[128,8]{0,1:T(8,128)} async-done(((f32[1024,8]{0,1:T(8,128)}), f32[128,8]{0,1:T(8,128)}) %reduce-scatter.13.cloned.1.call-update) | async-done | bytes 4112 | tf_op jit(solution)/shard_map/reduce_scatter | solution.py:118
  69.3 0.7 broadcast_multiply_fusion.2
  70.1 0.5 fusion.30
  72.1 0.6 fusion.27
  72.8 17.1 %multiply_add_fusion = f32[32,4,128,256]{3,2,1,0:T(8,128)} fusion(f32[32,4,128,256]{3,2,1,0:T(8,128)} %param.31, bf16[32,4,4,256]{3,1,2,0:T(4,128)(2,1)S(1)} %bitcast.83, f32[32,4]{1,0:T(8,128)S(1)} %copy.190, f32[32,4,4]{1,2,0:T(4,128)S(1)} %copy.191, bf16[32,4,512]{2,1,0:T(4,128)(2,1)S(1)} %copy-done.5), kind=kOutput, calls=%fused_computation.3 | convolution fusion | flops 209846272 | bytes 33950208 | tf_op jit(solution)/shard_map/sph,sphd,sphv->shdv/dot_general | solution.py:38
  89.9 50.2 %reduce-scatter.9.cloned.1.call-done = f32[128,512]{1,0:T(8,128)} async-done(((f32[1024,512]{1,0:T(8,128)}), f32[128,512]{1,0:T(8,128)}) %reduce-scatter.9.cloned.1.call-update) | async-done | bytes 262160 | tf_op jit(solution)/shard_map/reduce_scatter | solution.py:115
  140.1 70.9 %reduce-scatter.11.cloned.1.call-done = f32[128,512]{1,0:T(8,128)} async-done(((f32[1024,512]{1,0:T(8,128)}), f32[128,512]{1,0:T(8,128)}) %reduce-scatter.11.cloned.1.call-update) | async-done | bytes 262160 | tf_op jit(solution)/shard_map/reduce_scatter | solution.py:114
  211.1 1.1 broadcast_multiply_fusion.1
  212.3 1.0 fusion.23
  213.5 1.3 fusion.51
  215.1 86.8 %reduce-scatter.15.cloned.1.call-done = f32[128,1024]{1,0:T(8,128)} async-done(((f32[1024,1024]{1,0:T(8,128)}), f32[128,1024]{1,0:T(8,128)}) %reduce-scatter.15.cloned.1.call-update) | async-done | bytes 524304 | tf_op jit(solution)/shard_map/reduce_scatter | solution.py:117
  301.9 91.4 %reduce-scatter.7.cloned.1.call-done = f32[128,1024]{1,0:T(8,128)} async-done(((f32[1024,1024]{1,0:T(8,128)}), f32[128,1024]{1,0:T(8,128)}) %reduce-scatter.7.cloned.1.call-update) | async-done | bytes 524304 | tf_op jit(solution)/shard_map/reduce_scatter | solution.py:116
  393.4 1.4 broadcast_multiply_fusion
  395.3 1.2 convolution_bitcast_fusion.1
  396.6 11.8 %multiply_reduce_fusion = (f32[32,4,4]{1,2,0:T(4,128)S(1)}, f32[32,4,4,256]{3,1,2,0:T(4,128)S(1)}) fusion(f32[32,4,4]{1,2,0:T(4,128)S(1)} %copy.197, f32[32,4,4,256]{3,1,2,0:T(4,128)S(1)} %convolution_bitcast_fusion.1, f32[32,4,128,256]{3,2,1,0:T(8,128)} %multiply_add_fusion, f32[32,4,4,128]{3,2,1,0:T(4,128)S(1)} %reshape.113, f32[32,4,4]{1,2,0:T(4,128)S(1)} %copy.189), kind=kOutput, calls=%fused_computation.24 | convolution fusion | flops 201981440 | bytes 18094080 | tf_op jit(solution)/shard_map/sthd,shdv->sthv/dot_general | solution.py:60
  409.0 0.7 copy.208
  409.8 48.8 %all-gather.2.cloned.1.call-done = bf16[1024,1024]{1,0:T(8,128)(2,1)} async-done(((bf16[128,1024]{1,0:T(8,128)(2,1)}), bf16[1024,1024]{1,0:T(8,128)(2,1)}) %all-gather.2.cloned.1.call-update) | async-done | bytes 2097168 | tf_op jit(solution)/shard_map/all_gather | solution.py:152
  458.7 4.4 fusion.52
  463.1 29.9 %reduce-scatter.17.cloned.1.call-done = f32[256,512]{1,0:T(8,128)} async-done(((f32[1024,512]{1,0:T(8,128)}), f32[256,512]{1,0:T(8,128)}) %reduce-scatter.17.cloned.1.call-update) | async-done | bytes 524304 | tf_op jit(solution)/shard_map/reduce_scatter | solution.py:154
  493.0 1.8 convert_element_type.49
  (105 shorter events, 6.5 us)
Async XLA Ops:
  7.2 9.7 %copy-start = (bf16[512,1024]{1,0:T(8,128)(2,1)S(1)}, bf16[512,1024]{1,0:T(8,128)(2,1)}, u32[]{:S(2)}) copy-start(bf16[512,1024]{1,0:T(8,128)(2,1)} %param.26) | copy-start | bytes 3145732
  7.2 62.1 %reduce-scatter.13.cloned.1.call-start = ((), (), s32[]{:S(2)}) async-start(), calls=%async_computation.9 | async-start | bytes 36864 | tf_op jit(solution)/shard_map/reduce_scatter | solution.py:118
  11.1 3.7 copy-start.2
  11.1 3.7 copy-start.3
  11.1 129.0 %reduce-scatter.9.cloned.1.call-start = ((), (), s32[]{:S(2)}) async-start(), calls=%async_computation.7 | async-start | bytes 2359296 | tf_op jit(solution)/shard_map/reduce_scatter | solution.py:115
  14.7 196.4 %reduce-scatter.11.cloned.1.call-start = ((), (), s32[]{:S(2)}) async-start(), calls=%async_computation.8 | async-start | bytes 2359296 | tf_op jit(solution)/shard_map/reduce_scatter | solution.py:114
  16.9 285.1 %reduce-scatter.15.cloned.1.call-start = ((), (), s32[]{:S(2)}) async-start(), calls=%async_computation.10 | async-start | bytes 4718592 | tf_op jit(solution)/shard_map/reduce_scatter | solution.py:117
  20.1 373.3 %reduce-scatter.7.cloned.1.call-start = ((), (), s32[]{:S(2)}) async-start(), calls=%async_computation.6 | async-start | bytes 4718592 | tf_op jit(solution)/shard_map/reduce_scatter | solution.py:116
  24.6 0.7 copy-start.13
  24.6 0.7 copy-start.11
  24.7 0.7 copy-start.14
  24.7 0.8 copy-start.10
  24.7 0.8 copy-start.8
  24.7 0.8 copy-start.12
  24.7 1.2 copy-start.1
  24.7 433.9 %all-gather.2.cloned.1.call-start = ((), (), s32[]{:S(2)}) async-start(), calls=%async_computation.11 | async-start | bytes 2359296 | tf_op jit(solution)/shard_map/all_gather | solution.py:152
  25.5 189.4 %copy-start.9 = (f32[32,4]{0,1:T(4,128)}, f32[32,4]{0,1:T(4,128)S(1)}, u32[]{:S(2)}) copy-start(f32[32,4]{0,1:T(4,128)S(1)} %get-tuple-element.8) | copy-start | bytes 1540
  31.4 40.6 %copy-start.5 = (bf16[32,4,512]{2,1,0:T(4,128)(2,1)S(1)}, bf16[32,4,512]{2,1,0:T(4,128)(2,1)}, u32[]{:S(2)}) copy-start(bf16[32,4,512]{2,1,0:T(4,128)(2,1)} %param.34) | copy-start | bytes 393220
  31.4 41.2 %copy-start.6 = (f32[32,4,128]{2,1,0:T(4,128)S(1)}, f32[32,4,128]{2,1,0:T(4,128)}, u32[]{:S(2)}) copy-start(f32[32,4,128]{2,1,0:T(4,128)} %param.32) | copy-start | bytes 196612
  31.4 41.3 %copy-start.4 = (bf16[32,4,1024]{2,1,0:T(4,128)(2,1)S(1)}, bf16[32,4,1024]{2,1,0:T(4,128)(2,1)}, u32[]{:S(2)}) copy-start(bf16[32,4,1024]{2,1,0:T(4,128)(2,1)} %param.35) | copy-start | bytes 786436
  72.7 139.6 %copy-start.7 = (f32[32,4,128]{2,1,0:T(4,128)}, f32[32,4,128]{2,1,0:T(4,128)S(1)}, u32[]{:S(2)}) copy-start(f32[32,4,128]{2,1,0:T(4,128)S(1)} %multiply_add_fusion.1) | copy-start | bytes 196612
  409.8 83.2 %reduce-scatter.17.cloned.1.call-start = ((), (), s32[]{:S(2)}) async-start(), calls=%async_computation.12 | async-start | bytes 2621440 | tf_op jit(solution)/shard_map/reduce_scatter | solution.py:154
Sparse Core Ops, SparseCore 0:
  11.7 57.5 reduce-scatter.12
  72.8 67.3 reduce-scatter.8
  143.7 67.3 reduce-scatter.10
  214.6 87.3 reduce-scatter.14
  305.4 87.9 reduce-scatter.6
  409.9 48.6 all-gather.1
  463.2 29.7 reduce-scatter.16
where the time goes:
time: 502 us
  waiting for transfers between devices  392 us (78%)
  matrix products  53.4 us (11%)
  blocking collectives  23.3 us (5%)
  between operations  14.6 us (3%)
  local copies, waits for them, and re-layouts  11.9 us (2%)
  other arithmetic  6.63 us (1%)
    reduce_scatter x1, waiting for transfers between devices, per_device(): lax.psum_scatter(part_value, 'kv', scatter_dimension=0, tiled=True)  91.4 us
    reduce_scatter x1, waiting for transfers between devices, per_device(): lax.psum_scatter(part_outgate, 'kv', scatter_dimension=0, tiled=True)  86.8 us
    reduce_scatter x1, waiting for transfers between devices, per_device(): lax.psum_scatter(part_query, 'kv', scatter_dimension=0, tiled=True)  70.9 us
    reduce_scatter x1, waiting for transfers between devices, per_device(): lax.psum_scatter(part_key, 'kv', scatter_dimension=0, tiled=True)  50.2 us
    all_gather x1, waiting for transfers between devices, per_device(): lax.all_gather(hidden, 'kv', axis=0, tiled=True)  48.8 us
    reduce_scatter x1, waiting for transfers between devices, per_device(): lax.psum_scatter(partial_out, 'tp', scatter_dimension=0, tiled=True)  29.9 us
    psum x1, blocking collectives, per_device(): all_squares = lax.psum(part_squares, 'kv')  23.3 us
    dot_general x1, matrix products, commit(): jnp.einsum('sph,sphd,sphv->shdv', weights, prior_k, prior_v, precision=hp)  17.1 us
  transfers between devices with their start and end apart: 7, of which 7 were waited for; matrix products, arithmetic and copies ran while one was open for 9% of the time, Pallas kernels for 0%

commit v1 on v0

v1 whole, which is shorter than its diff:
```python
import functools

import jax
import jax.numpy as jnp
from jax import lax
from jax.experimental import pallas as pl
from jax.experimental.pallas import tpu as pltpu
from jax.sharding import PartitionSpec as P


D = 4096
HEADS = 16
DQK = 128
DV = 256
PROP = 4
PLAN = ((3, False), (3, False), (2, False))
ORDER = ("g0", "p1", "o0", "m0", "p2", "f0", "m1", "s0", "m2", "f1", "w0", "r0", "f2", "c0", "c1", "r1", "r2")
COMMITS = (2, 2, 2, 2)
OUTPUTS = ((0, 1), (2,))
SPREAD_AFTER = (("c0", "r1"), ("r2", "r2"), ("r2",))
TOKEN = (8, 128)
VMEM_LIMIT = 20 * 1024 * 1024
VMEM_MOST = 48 * 1024 * 1024
VMEM_ALL = 60 * 1024 * 1024


F32 = jnp.float32
BF16 = jnp.bfloat16
HIGHEST = lax.Precision.HIGHEST


def commit(normal, stable, prior_k, prior_i, prior_f, accepted):
    count = prior_k.shape[1]
    live = (jnp.arange(count, dtype=jnp.int32)[None, :] < accepted[:, None])[:, :, None]
    forget_live = jnp.where(live, prior_f, 0.0)
    parts = [forget_live[:, 0]]
    for s in range(1, count):
        parts.append(parts[-1] + forget_live[:, s])
    cumul = jnp.stack(parts, axis=1)
    total = parts[-1]
    weight_log = jnp.where(live, total[:, None, :] - cumul + prior_i, -jnp.inf)
    new_stable = jnp.maximum(total + stable, jnp.max(weight_log, axis=1))
    weights = jnp.exp(weight_log - new_stable[:, None, :])
    decay = jnp.exp(total + stable - new_stable)
    new_normal = decay[:, :, None] * normal + jnp.einsum(
        "sph,sphd->shd", weights, prior_k, precision=HIGHEST
    )
    return (decay, weights, new_normal, new_stable)


def commit_body(mat_ref, left_ref, right_ref, decay_ref, *refs):
    out_ref, token_ref = refs[-2:]
    token_ref[...] = jnp.zeros_like(token_ref)
    seqs, head_local = mat_ref.shape[:2]
    for s in range(seqs):
        for h in range(head_local):
            added = lax.dot_general(
                left_ref[s, :, h * DQK : (h + 1) * DQK],
                right_ref[s, :, h * DV : (h + 1) * DV],
                (((0,), (0,)), ((), ())),
                preferred_element_type=F32,
            )
            out_ref[s, h] = decay_ref[s, :, h : h + 1] * mat_ref[s, h] + added


def commit_factors(prior_k, prior_v, weights):
    key = prior_k.astype(F32) * jnp.repeat(weights, DQK, axis=2)
    high = key.astype(BF16)
    rest = key - high.astype(F32)
    middle = rest.astype(BF16)
    low = (rest - middle.astype(F32)).astype(BF16)
    left = jnp.concatenate([high, middle, low, jnp.zeros_like(low)], axis=1)
    right = jnp.concatenate([prior_v, prior_v, prior_v, jnp.zeros_like(prior_v)], axis=1)
    return left, right


def commit_matrix(first, count, matrix, left, right, decay, before, after):
    head_local = matrix.shape[1]
    step = 4 if count % 4 == 0 and first % 4 == 0 else 1
    start = first // step
    block = pl.BlockSpec((step,) + matrix.shape[1:], lambda s: (start + s, 0, 0, 0))
    rows = lambda array: pl.BlockSpec((step,) + array.shape[1:], lambda s: (start + s, 0, 0))
    anywhere = pl.BlockSpec(memory_space=pl.ANY)
    operands = [matrix, left, right, decay, after]
    specs = [block, rows(left), rows(right), rows(decay), anywhere]
    aliases = {}
    if before is not None:
        aliases = {len(operands): 0}
        operands.append(before)
        specs.append(anywhere)
    return pl.pallas_call(
        commit_body,
        grid=(count // step,),
        in_specs=specs,
        out_specs=[block, full_spec(TOKEN)],
        out_shape=[jax.ShapeDtypeStruct(matrix.shape, F32), jax.ShapeDtypeStruct(TOKEN, F32)],
        input_output_aliases=aliases,
        compiler_params=pltpu.CompilerParams(vmem_limit_bytes=VMEM_ALL),
        cost_estimate=pl.CostEstimate(
            flops=32 * count * head_local * left.shape[1] * DQK * DV,
            bytes_accessed=8 * count * head_local * DQK * DV,
            transcendentals=0,
        ),
        name="commit_matrix",
    )(*operands)


def small_body(head_local, pos_ref, x_ref, gain_ref, gate_ref, _, keep_ref, send_ref):
    kv_at = pos_ref[0]
    count, rows, width = x_ref.shape
    half = count // 2
    nt = (((1,), (1,)), ((), ()))
    index = lax.broadcasted_iota(jnp.int32, (16, 2 * HEADS), 0)
    column = lax.broadcasted_iota(jnp.int32, (16, 2 * HEADS), 1)
    wanted = jnp.where(index < head_local, index, index - head_local + HEADS)
    pick = (index < 2 * head_local) & (column == wanted + pos_ref[1] * head_local)
    last = lax.broadcasted_iota(jnp.int32, (16, rows), 0) == 2 * head_local
    ones = jnp.ones((16, width), BF16)
    for k in range(count):
        x = x_ref[k].astype(F32)
        normed = (x * gain_ref[...]).astype(BF16)
        gates = lax.dot_general(gate_ref[...], normed, nt, preferred_element_type=F32)
        own = jnp.dot(pick.astype(F32), gates, precision=HIGHEST, preferred_element_type=F32)
        square = x * x
        high = square.astype(BF16)
        low = (square - high.astype(F32)).astype(BF16)
        squares = lax.dot_general(ones, high, nt, preferred_element_type=F32) + lax.dot_general(
            ones, low, nt, preferred_element_type=F32
        )
        value = jnp.where(last, squares, own)
        apart = jnp.bitwise_xor(kv_at, k)
        place = lax.rem(apart, half)

        @pl.when(apart < half)
        def _():
            keep_ref[place] = value

        @pl.when(apart >= half)
        def _():
            send_ref[place] = value


def small_sums(pos, blocks, gain, gate_weight, head_local, after):
    count, rows, width = blocks.shape
    shape = (count // 2, 16, rows)
    assert 2 * head_local < 16
    return pl.pallas_call(
        functools.partial(small_body, head_local),
        grid_spec=pltpu.PrefetchScalarGridSpec(
            num_scalar_prefetch=1,
            grid=(1,),
            in_specs=[
                full_spec(blocks.shape),
                pl.BlockSpec((None, 1, width), lambda i, pos_ref: (pos_ref[0], 0, 0)),
                full_spec((gate_weight.shape[1], width)),
                pl.BlockSpec(memory_space=pl.ANY),
            ],
            out_specs=[full_spec(shape), full_spec(shape)],
        ),
        out_shape=[jax.ShapeDtypeStruct(shape, F32)] * 2,
        compiler_params=pltpu.CompilerParams(vmem_limit_bytes=VMEM_LIMIT),
        cost_estimate=pl.CostEstimate(
            flops=100 * count * rows * width, bytes_accessed=2 * count * rows * width, transcendentals=0
        ),
        name="small_sums",
    )(pos, blocks, gain, gate_weight.T, after)


def paths_body(head_local, pos_ref, near_ref, far_ref, bias_ref, parent_ref, stable_ref, decay_ref, _, wmat_ref, cols_ref):
    rows = near_ref.shape[1]
    total = near_ref[...] + far_ref[...]
    row = lax.broadcasted_iota(jnp.int32, (rows, rows), 0)
    lane = lax.broadcasted_iota(jnp.int32, (rows, rows), 1)
    same = row == lane
    parent = parent_ref[...]
    link = ((parent >= 0) & (lane == row // PROP * PROP + parent)).astype(BF16)
    path = (same.astype(F32) + link.astype(F32)).astype(BF16)
    power = link
    reach = 2
    while reach < PROP:
        power = jnp.dot(power, power, preferred_element_type=F32).astype(BF16)
        path = path + jnp.dot(power, path, preferred_element_type=F32).astype(BF16)
        reach *= 2
    path = path.astype(F32)
    on_path = path > 0.5
    scale_row = lax.rsqrt(total[2 * head_local : 2 * head_local + 1] / D + 1e-06)
    scale = jnp.sum(jnp.where(same, scale_row, 0.0), axis=1, keepdims=True)
    for h in range(head_local):
        ingate = total[h : h + 1] * scale_row
        bias = bias_ref[pos_ref[1] * head_local + h]
        raw = total[head_local + h : head_local + h + 1] * scale_row + bias
        logforget = jnp.minimum(raw, 0.0) - jnp.log1p(jnp.exp(-jnp.abs(raw)))
        path_sum = jnp.sum(path * logforget, axis=1, keepdims=True)
        path_row = jnp.sum(jnp.where(same, path_sum, 0.0), axis=0, keepdims=True)
        dlog = jnp.where(on_path, path_sum - path_row + ingate, -jnp.inf)
        carried = path_sum + stable_ref[:, h : h + 1]
        top = jnp.maximum(carried, jnp.max(dlog, axis=1, keepdims=True))
        wmat_ref[h] = jnp.exp(dlog - top) / jnp.sqrt(F32(DQK))
        cols_ref[h, :, 0:1] = scale
        factor = jnp.exp(carried - top)
        cols_ref[h, :, 1:2] = factor
        cols_ref[h, :, 3:4] = factor * decay_ref[:, h : h + 1]
        cols_ref[h, :, 2:3] = jnp.exp(-top)


def path_weights(pos, near, far, bias, parents, stable_rows, decay_rows, head_local, after):
    rows = near.shape[1]
    shapes = [(head_local, rows, rows), (head_local, rows, 4)]
    return pl.pallas_call(
        functools.partial(paths_body, head_local),
        grid_spec=pltpu.PrefetchScalarGridSpec(
            num_scalar_prefetch=1,
            grid=(1,),
            in_specs=[
                full_spec(near.shape),
                full_spec(far.shape),
                pl.BlockSpec(memory_space=pltpu.SMEM),
                full_spec((rows, 1)),
                full_spec(stable_rows.shape),
                full_spec(decay_rows.shape),
                pl.BlockSpec(memory_space=pl.ANY),
            ],
            out_specs=[full_spec(shape) for shape in shapes],
        ),
        out_shape=[jax.ShapeDtypeStruct(shape, F32) for shape in shapes],
        compiler_params=pltpu.CompilerParams(vmem_limit_bytes=VMEM_LIMIT),
        cost_estimate=pl.CostEstimate(
            flops=20 * head_local * rows * rows, bytes_accessed=4 * head_local * rows * rows, transcendentals=0
        ),
        name="path_weights",
    )(pos, near, far, bias, parents.reshape(rows, 1), stable_rows, decay_rows, after)


HEAD_COLS = 2 * DQK + 2 * DV


def full_spec(shape):
    return pl.BlockSpec(shape, lambda i, *_: (0,) * len(shape))


def normed_rows(x_refs, gain_ref, normed_ref):
    at = 0
    for x_ref in x_refs:
        rows = x_ref.shape[0]
        normed_ref[at : at + rows] = (x_ref[...].astype(F32) * gain_ref[...]).astype(BF16)
        at += rows


def project_body(count, pos_ref, *refs):
    x_refs = refs[:count]
    gain_ref, wq_ref, wk_ref, wv_ref, wg_ref, _ = refs[count : count + 6]
    out_refs = refs[count + 6 : -1]
    normed_ref = refs[-1]

    @pl.when(pl.program_id(0) == 0)
    def _():
        normed_rows(x_refs, gain_ref, normed_ref)

    at = 0
    for w_ref in (wq_ref, wk_ref, wv_ref, wg_ref):
        width = w_ref.shape[1]
        product = jnp.dot(normed_ref[...], w_ref[...], preferred_element_type=F32)
        row = 0
        for out_ref in out_refs:
            rows = out_ref.shape[0]
            out_ref[:, at : at + width] = product[row : row + rows].astype(out_ref.dtype)
            row += rows
        at += width


def project(pos, tokens, gain, weights, pieces, dtype, head_local, after, limit):
    width = tokens.shape[2]

    def block(j, offset, rows):
        return pl.BlockSpec(
            (None, rows, width),
            lambda h, pos_ref: (jnp.bitwise_xor(pos_ref[0], j), offset // rows, 0),
        )

    specs = [block(j, offset, rows) for offset, rows, order in pieces for j in order]
    count = len(specs)
    specs.append(pl.BlockSpec((None, 1, width), lambda h, pos_ref: (pos_ref[0], 0, 0)))
    for cols in (DQK, DQK, DV, DV):
        specs.append(pl.BlockSpec((width, cols), lambda h, pos_ref: (0, h)))
    specs.append(pl.BlockSpec(memory_space=pl.ANY))
    outs = [rows * len(order) for _, rows, order in pieces]
    total = sum(outs)
    cols = head_local * HEAD_COLS
    return pl.pallas_call(
        functools.partial(project_body, count),
        grid_spec=pltpu.PrefetchScalarGridSpec(
            num_scalar_prefetch=1,
            grid=(head_local,),
            in_specs=specs,
            out_specs=[pl.BlockSpec((out, HEAD_COLS), lambda h, pos_ref: (0, h)) for out in outs],
            scratch_shapes=[pltpu.VMEM((total, width), BF16)],
        ),
        out_shape=[jax.ShapeDtypeStruct((out, cols), dtype) for out in outs],
        compiler_params=pltpu.CompilerParams(vmem_limit_bytes=limit),
        cost_estimate=pl.CostEstimate(
            flops=2 * total * width * cols,
            bytes_accessed=2 * (total + width) * cols,
            transcendentals=0,
        ),
        name="project_other" if dtype == BF16 else "project_own",
    )(pos, *([tokens] * count), gain, *weights, after)


def fold_body(keep_ref, other_ref, _, out_ref, send_ref, token_ref):
    token_ref[...] = jnp.zeros_like(token_ref)
    rows = out_ref.shape[0]
    out_ref[...] = keep_ref[:rows] + other_ref[:rows].astype(F32)
    send_ref[...] = (keep_ref[rows:] + other_ref[rows:].astype(F32)).astype(BF16)


def fold(keep, other, head_local, after):
    count, cols = keep.shape
    spec = lambda rows: pl.BlockSpec((rows, HEAD_COLS), lambda h: (0, h))
    return pl.pallas_call(
        fold_body,
        grid=(head_local,),
        in_specs=[spec(count), spec(count), pl.BlockSpec(memory_space=pl.ANY)],
        out_specs=[spec(count // 2), spec(count // 2), full_spec(TOKEN)],
        out_shape=[
            jax.ShapeDtypeStruct((count // 2, cols), F32),
            jax.ShapeDtypeStruct((count // 2, cols), BF16),
            jax.ShapeDtypeStruct(TOKEN, F32),
        ],
        compiler_params=pltpu.CompilerParams(vmem_limit_bytes=VMEM_LIMIT),
        cost_estimate=pl.CostEstimate(
            flops=2 * count * cols, bytes_accessed=9 * count * cols, transcendentals=0
        ),
        name="fold",
    )(keep, other, after)


def read_body(head_local, first_seq, own_ref, *refs):
    got_ref, mat_ref, norm_ref, wmat_ref, cols_ref, key_ref, value_ref, weight_ref, gain_ref, _, hid_ref, token_ref = refs
    token_ref[...] = jnp.zeros_like(token_ref)
    rows = own_ref.shape[0]
    seqs = mat_ref.shape[0]
    prop = rows // seqs
    all_seqs = norm_ref.shape[1]
    row_seq = first_seq + lax.broadcasted_iota(jnp.int32, (rows, all_seqs), 0) // prop
    pick = (row_seq == lax.broadcasted_iota(jnp.int32, (rows, all_seqs), 1)).astype(F32)
    lane_seq = lax.broadcasted_iota(jnp.int32, (rows, seqs * DQK), 1) // DQK
    big_seq = lax.broadcasted_iota(jnp.int32, (rows, seqs * DQK), 0) // prop
    big_pick = lane_seq == big_seq
    together = (
        lax.broadcasted_iota(jnp.int32, (rows, rows), 0) // prop
        == lax.broadcasted_iota(jnp.int32, (rows, rows), 1) // prop
    )
    nt = (((1,), (1,)), ((), ()))
    for h in range(head_local):
        base = h * HEAD_COLS

        def total(at, width):
            cols = slice(base + at, base + at + width)
            return own_ref[:, cols] + got_ref[:, cols].astype(F32)

        scale = cols_ref[h, :, 0:1]
        factor = cols_ref[h, :, 1:2]
        floor = cols_ref[h, :, 2:3]
        decayed = cols_ref[h, :, 3:4]
        query = scale * total(0, DQK)
        key = scale * total(DQK, DQK)
        value = scale * total(2 * DQK, DV)
        gate = scale * total(2 * DQK + DV, DV)
        scores = (
            lax.dot_general(query, key, nt, precision=HIGHEST, preferred_element_type=F32)
            * wmat_ref[h]
        )
        numer = jnp.dot(scores, value, precision=HIGHEST, preferred_element_type=F32)
        spread = jnp.where(big_pick, jnp.concatenate([query] * seqs, axis=1), 0.0).astype(BF16)
        mat = mat_ref[:, h].reshape(seqs * DQK, DV).astype(BF16)
        saved = jnp.dot(spread, mat, preferred_element_type=F32)
        prior_key = key_ref[:, h * DQK : (h + 1) * DQK].astype(F32)
        prior = lax.dot_general(query, prior_key, nt, precision=HIGHEST, preferred_element_type=F32)
        prior = jnp.where(together, prior * weight_ref[h : h + 1], 0.0)
        prior_value = value_ref[:, h * DV : (h + 1) * DV].astype(F32)
        added = jnp.dot(prior, prior_value, precision=HIGHEST, preferred_element_type=F32)
        qn = lax.dot_general(query, norm_ref[h], nt, precision=HIGHEST, preferred_element_type=F32)
        denom = jnp.sum(scores, axis=1, keepdims=True) + factor * jnp.sum(
            qn * pick, axis=1, keepdims=True
        )
        read = (numer + decayed * saved + factor * added) / jnp.maximum(jnp.abs(denom), floor)
        normer = lax.rsqrt(jnp.mean(read * read, axis=1, keepdims=True) + 1e-06)
        gain = gain_ref[:, h * DV : (h + 1) * DV]
        hid_ref[:, h * DV : (h + 1) * DV] = (
            read * normer * gain * jax.nn.sigmoid(gate)
        ).astype(BF16)


def tree_read(offset, own, got, mat, norm, wmat, cols, prior, gain, head_local, after):
    rows = own.shape[0]
    seqs = rows // PROP
    keys, values, weights = prior
    return pl.pallas_call(
        functools.partial(read_body, head_local, offset // PROP),
        grid=(1,),
        in_specs=[full_spec(own.shape), full_spec(got.shape)]
        + [
            pl.BlockSpec((seqs,) + mat.shape[1:], lambda i: (offset // rows, 0, 0, 0)),
            full_spec(norm.shape),
            full_spec(wmat.shape),
            pl.BlockSpec((head_local, rows, cols.shape[2]), lambda i: (0, offset // rows, 0)),
            pl.BlockSpec((rows, keys.shape[1]), lambda i: (offset // rows, 0)),
            pl.BlockSpec((rows, values.shape[1]), lambda i: (offset // rows, 0)),
            full_spec(weights.shape),
            full_spec(gain.shape),
            pl.BlockSpec(memory_space=pl.ANY),
        ],
        out_specs=[full_spec((rows, head_local * DV)), full_spec(TOKEN)],
        out_shape=[
            jax.ShapeDtypeStruct((rows, head_local * DV), BF16),
            jax.ShapeDtypeStruct(TOKEN, F32),
        ],
        compiler_params=pltpu.CompilerParams(vmem_limit_bytes=VMEM_MOST),
        cost_estimate=pl.CostEstimate(
            flops=8 * rows * seqs * head_local * DQK * DV,
            bytes_accessed=4 * seqs * head_local * DQK * DV,
            transcendentals=0,
        ),
        name="tree_read",
    )(own, got, mat, norm, wmat, cols, keys, values, weights, gain, after)


def output_body(orders, pos_ref, *refs):
    w_ref = refs[sum(len(order) for order in orders)]
    keep_ref, send_ref = refs[-2:]
    kv_at = pos_ref[0]
    tp_at = pos_ref[1]
    weight = w_ref[...]
    ref_at = 0
    offset = 0
    for order in orders:
        rows = refs[ref_at].shape[0]
        span = slice(offset, offset + rows)
        for distances in order:
            out = jnp.dot(refs[ref_at][...], weight, preferred_element_type=F32)
            ref_at += 1
            for i, j in enumerate(distances):
                piece = out[i * rows : (i + 1) * rows]
                block = jnp.bitwise_xor(kv_at, j)
                apart = jnp.bitwise_xor(lax.div(block, 2), tp_at)
                side = lax.rem(block, 2)
                place = lax.div(apart, 2)
                here = lax.rem(apart, 2) == 0

                @pl.when(here)
                def _():
                    keep_ref[place, side, span] = piece

                @pl.when(jnp.logical_not(here))
                def _():
                    send_ref[place, side, span] = piece

        offset += rows


def output_product(pos, groups, weight, after, tp_size):
    orders = tuple(tuple(distances for distances, _ in group) for group in groups)
    rows = sum(group[0][1].shape[0] for group in groups)
    flat = [value for group in groups for _, value in group]
    shape = (tp_size // 2, 2, rows, weight.shape[1])
    return pl.pallas_call(
        functools.partial(output_body, orders),
        grid_spec=pltpu.PrefetchScalarGridSpec(
            num_scalar_prefetch=1,
            grid=(1,),
            in_specs=[full_spec(value.shape) for value in flat]
            + [full_spec(weight.shape)]
            + [pl.BlockSpec(memory_space=pl.ANY)] * len(after),
            out_specs=[full_spec(shape), full_spec(shape)],
        ),
        out_shape=[jax.ShapeDtypeStruct(shape, F32)] * 2,
        compiler_params=pltpu.CompilerParams(vmem_limit_bytes=VMEM_LIMIT),
        cost_estimate=pl.CostEstimate(
            flops=4 * tp_size * rows * weight.shape[0] * weight.shape[1],
            bytes_accessed=2 * weight.shape[0] * weight.shape[1],
            transcendentals=0,
        ),
        name="output_product",
    )(pos, *flat, weight, *after)


def per_device(
    kv_size,
    tp_size,
    tokens,
    norm_gain,
    query_weight,
    key_weight,
    value_weight,
    outgate_weight,
    gate_weight,
    forget_bias,
    head_gain,
    output_weight,
    state_matrix,
    state_normal,
    state_stable,
    prior_keys,
    prior_values,
    prior_ingate,
    prior_forget,
    accepted,
    parents,
):
    head_local = query_weight.shape[1] // DQK
    width_local = tokens.shape[1]
    seq_local = accepted.shape[0]
    row_local = seq_local * PROP
    unit = row_local // sum(share for share, _ in PLAN)
    bits = [1 << i for i in range(kv_size.bit_length() - 1)]
    chunks = []
    for share, along_z in PLAN:
        steps = bits[1:] + bits[:1] if along_z else bits
        chunks.append((sum(rows for _, rows, _ in chunks), share * unit, steps))
    kv_at = lax.axis_index("kv")
    tp_at = lax.axis_index("tp")
    pos = jnp.stack([kv_at, tp_at]).astype(jnp.int32)

    def swap(value, axis, size, bit):
        return lax.ppermute(value, axis, [(i, i ^ bit) for i in range(size)])

    def across(value, bit):
        return swap(value, "kv", kv_size, bit)

    def near_first(steps):
        order = [0]
        for bit in reversed(steps):
            order = order + [j ^ bit for j in order]
        return order

    weights = (query_weight, key_weight, value_weight, outgate_weight)
    blocks = tokens.reshape(kv_size, row_local, width_local)
    gain_blocks = norm_gain.reshape(kv_size, 1, width_local)

    def project_first(c, after):
        offset, rows, steps = chunks[c]
        order = [j ^ steps[0] for j in near_first(steps[1:])]
        (sent,) = project(
            pos, blocks, gain_blocks, weights, [(offset, rows, order)], BF16, head_local, after,
            VMEM_ALL if c == 0 else VMEM_LIMIT,
        )
        return sent

    count = len(chunks)
    first_sent = project_first(0, pos)
    came = [across(first_sent, chunks[0][2][0])] + [None] * (count - 1)

    token = first_sent
    own = [None] * count
    got = [None] * count
    hidden = [None] * count
    done = {}
    matrices = []

    def run_commit(index, after):
        portion = seq_local // sum(COMMITS)
        factors = commit_factors(prior_keys, prior_values, commit_weights)
        matrix, after = commit_matrix(
            portion * sum(COMMITS[:index]), portion * COMMITS[index], state_matrix, *factors, decay[:, None, :],
            matrices[-1] if matrices else None, after,
        )
        matrices.append(matrix)
        return after

    def prepare(after):
        zero = after[0, 0]
        prior_f32 = prior_keys.astype(F32).reshape(seq_local, PROP, head_local, DQK)
        decay, commit_weights, new_normal, new_stable = commit(
            state_normal, state_stable + zero, prior_f32, prior_ingate, prior_forget + zero, accepted
        )
        return decay, commit_weights, new_normal, new_stable

    gain = head_gain[None, :]

    for event in ORDER:
        kind, c = event[0], int(event[1])
        offset, rows, steps = chunks[c]
        if kind == "g":
            small, away = small_sums(pos, blocks, gain_blocks, gate_weight, head_local, token)
            token = small
            for bit in reversed(bits[1:]):
                total = small + across(away, bit)
                left = total.shape[0] // 2
                small, away = total[:left], total[left:]
            small_far = across(away[0], bits[0])
            small_near = small[0]
        elif kind == "p":
            token = project_first(c, token)
            came[c] = across(token, steps[0])
        elif kind == "o":
            pieces = [(offset, rows, near_first(steps[1:])) for offset, rows, steps in chunks]
            own = project(pos, blocks, gain_blocks, weights, pieces, F32, head_local, token, VMEM_LIMIT)
            own = list(own)
            token = own[0]
        elif kind == "m":
            own[c], send, token = fold(own[c], came[c], head_local, token)
            got[c] = across(send, steps[1])
        elif kind == "s":
            decay, commit_weights, new_normal, new_stable = prepare(token)
            normal_heads = new_normal.transpose(1, 0, 2)
            stable_rows = jnp.repeat(new_stable, PROP, axis=0)
            decay_rows = jnp.repeat(decay, PROP, axis=0)
            prior_rows = (
                prior_keys.reshape(row_local, -1),
                prior_values.reshape(row_local, -1),
                commit_weights.reshape(row_local, head_local).T,
            )
        elif kind == "c":
            token = run_commit(c, token)
        elif kind == "w":
            wmat, cols = path_weights(
                pos, small_near, small_far, forget_bias, parents, stable_rows, decay_rows, head_local, token
            )
            token = cols
        elif kind == "f":
            for bit in steps[2:]:
                own[c], send, token = fold(own[c], got[c], head_local, token)
                got[c] = across(send, bit)
        else:
            span = slice(offset, offset + rows)
            keys, values, weight_row = prior_rows
            hidden[c], token = tree_read(
                offset, own[c], got[c], state_matrix, normal_heads, wmat[:, span, span], cols,
                (keys, values, weight_row[:, span]), gain, head_local, token,
            )
        done[event] = token

    def reduce_out(keep, send):
        got = swap(send, "tp", tp_size, 1)
        total = keep + got
        bit = 2
        while bit < tp_size:
            away = total[1::2].astype(BF16)
            if bit == 2:
                leaving.append(away)
            got = swap(away, "tp", tp_size, bit)
            total = total[::2] + got.astype(F32)
            bit *= 2
        return total[0].astype(BF16)

    def spread(c):
        group = [((0,), hidden[c])]
        if c < count - 1:
            steps = [[bit] for bit in reversed(bits)]
        else:
            steps = [near_first(bits[1:])[1:], [bits[0]]]
        for index, apart in enumerate(steps):
            reach = tuple(j for distances, _ in group for j in distances)
            values = [value for _, value in group]
            have = values[0] if len(values) == 1 else jnp.concatenate(values, axis=0)
            if index > 0:
                last = min(index, len(SPREAD_AFTER[c])) - 1
                have = have + done[SPREAD_AFTER[c][last]][:1, :1].astype(BF16)
            joined[c] = have
            for bit in apart:
                group.append((tuple(j ^ bit for j in reach), across(have, bit)))
        return group

    joined = {}
    leaving = []
    groups = [spread(c) for c in range(count)]
    pieces = []
    while len(matrices) + 1 < len(COMMITS):
        token = run_commit(len(matrices), token)
    for part in OUTPUTS:
        keep, send = output_product(
            pos, [groups[c] for c in part], output_weight, [token] + [joined[c] for c in joined], tp_size
        )
        token = keep
        pieces.append(reduce_out(keep, send))
    run_commit(len(matrices), leaving[-1] if leaving else token)
    new_matrix = matrices[-1]
    layer_out = jnp.concatenate(pieces, axis=1).reshape(2 * row_local, -1)
    return (layer_out, new_matrix, new_normal, new_stable)


def solution(mesh):
    placed = (
        P(None, "kv"),
        P(),
        P("kv", "tp"),
        P("kv", "tp"),
        P("kv", "tp"),
        P("kv", "tp"),
        P("kv", None),
        P(),
        P("tp"),
        P("tp", "kv"),
        P("kv", "tp", None, None),
        P("kv", "tp", None),
        P("kv", "tp"),
        P("kv", None, "tp"),
        P("kv", None, "tp"),
        P("kv", None, "tp"),
        P("kv", None, "tp"),
        P("kv"),
        P("kv", None),
    )
    kv_size = mesh.shape["kv"]
    tp_size = mesh.shape["tp"]
    assert kv_size == 2 * tp_size

    def layered(*args):
        return per_device(kv_size, tp_size, *args)

    return jax.shard_map(
        layered,
        mesh=mesh,
        in_specs=placed,
        out_specs=(P("tp", "kv"), P("kv", "tp", None, None), P("kv", "tp", None), P("kv", "tp")),
        check_vma=False,
    )
```

time: 502 us -> 191 us (0.38)
  waiting for transfers between devices: 392 us -> 37 us
  Pallas kernels: 0 us -> 70.9 us
  matrix products: 53.4 us -> 1.19 us
  starting transfers between devices: 0.29 us -> 35.8 us
  blocking collectives: 23.3 us -> 0 us
  local copies, waits for them, and re-layouts: 11.9 us -> 31.3 us
  between operations: 14.6 us -> 1.28 us
  other arithmetic: 6.63 us -> 12.3 us
    reduce_scatter x6 -> x0, waiting for transfers between devices: 343 us -> none  [the longest x1 91.4 us: per_device(): lax.psum_scatter(part_value, 'kv', scatter_dimension=0, tiled=True)]
    pallas_call x0 -> x21, Pallas kernels: none -> 70.9 us  [the longest x4 17.1 us: project(): pl.pallas_call(functools.partial(project_body, count), grid_spec=pltpu.Pr...]
    dot_general x13 -> x1, matrix products: 53.4 us -> 1.19 us  [commit(): jnp.einsum('sph,sphd->shd', weights, prior_k, precision=HIGHEST)]
    all_gather x1 -> x0, waiting for transfers between devices: 48.8 us -> none  [per_device(): lax.all_gather(hidden, 'kv', axis=0, tiled=True)]
    ppermute x0 -> x26, waiting for transfers between devices: none -> 37 us  [swap(): return lax.ppermute(value, axis, [(i, i ^ bit) for i in range(size)])]
    ppermute x0 -> x26, starting transfers between devices: none -> 35.8 us  [swap(): return lax.ppermute(value, axis, [(i, i ^ bit) for i in range(size)])]
    psum x1 -> x0, blocking collectives: 23.3 us -> none  [per_device(): all_squares = lax.psum(part_squares, 'kv')]
    unnamed x31 -> x120, local copies, waits for them, and re-layouts: 1.35 us -> 21.7 us
  transfers between devices with their start and end apart: 7 -> 26, of which waited for: 7 -> 8; matrix products, arithmetic and copies ran while one was open for 9% -> 12% of each run, Pallas kernels for 0% -> 32%
where the time goes in v1:
time: 191 us; the launch traced here: 190 us
  Pallas kernels  70.9 us (37%)
  waiting for transfers between devices  37 us (19%)
  starting transfers between devices  35.8 us (19%)
  local copies, waits for them, and re-layouts  31.3 us (16%)
  other arithmetic  12.3 us (6%)
    ppermute x26, waiting for transfers between devices, swap(): return lax.ppermute(value, axis, [(i, i ^ bit) for i in range(size)])  37 us
    ppermute x26, starting transfers between devices, swap(): return lax.ppermute(value, axis, [(i, i ^ bit) for i in range(size)])  35.8 us
    unnamed x120, local copies, waits for them, and re-layouts  21.7 us
    pallas_call x4, Pallas kernels, project(): pl.pallas_call(functools.partial(project_body, count), grid_spec=pltpu.Pr...  17.1 us
    pallas_call x4, Pallas kernels, commit_matrix(): pl.pallas_call(commit_body, grid=(count // step,), in_specs=specs, out_sp...  16.8 us
    pallas_call x3, Pallas kernels, tree_read(): pl.pallas_call(functools.partial(read_body, head_local, offset // PROP),...  13.1 us
    pallas_call x6, Pallas kernels, fold(): pl.pallas_call(fold_body, grid=(head_local,), in_specs=[spec(count), spec...  11.6 us
    pallas_call x2, Pallas kernels, output_product(): pl.pallas_call(functools.partial(output_body, orders), grid_spec=pltpu.Pr...  6.13 us
  transfers between devices with their start and end apart: 26, of which 8 were waited for; matrix products, arithmetic and copies ran while one was open for 12% of the time, Pallas kernels for 32%

profile of v1, /device:TPU:0, one launch (start us, length us, event | category | flops | bytes accessed | tf_op | source)
XLA Modules:
  0.0 189.7 jit_solution(522165097330892475)
XLA Ops:
  1.3 5.6 %project_other.3._ = bf16[192,3072]{1,0:T(8,128)(2,1)} custom-call(s32[2]{0:T(128)} %pad_add_fusion.pos_ref.refs_9_, bf16[8,128,512]{2,1,0:T(8,128)(2,1)} %bitcast.41, bf16[8,128,512]{2,1,0:T(8,128)(2,1)} %bitcast.42, bf16[8,128,512]{2,1,0:T(8,128)(2,1)} %bitcast.43, bf16[8,128,512]{2,1,0:T(8,128)(2,1)} %bitcast.44, f32[8,1,512]{2,1,0:T(1,128)} %bitcast.69, ...), custom_call_target="tpu_custom_call" | custom-call | flops 603979776 | bytes 4325376 | tf_op jit(solution)/shard_map/project_other/pallas_call | solution.py:289
  6.9 3.1 %collective-permute-start = (bf16[192,3072]{1,0:T(8,128)(2,1)}, bf16[192,3072]{1,0:T(8,128)(2,1)S(1)}, u32[]{:S(2)}, u32[]{:S(2)}) collective-permute-start(bf16[192,3072]{1,0:T(8,128)(2,1)} %project_other.3._), channel_id=1, source_target_pairs={{0,4},{4,0},{8,12},{12,8},{16,20},{20,16},{24,28},{28,24},{1,5},{5... | collective-permute-start | bytes 3538952 | tf_op jit(solution)/shard_map/ppermute | solution.py:525
  11.3 4.0 %small_sums.1 = (f32[4,16,128]{2,1,0:T(8,128)S(1)}, f32[4,16,128]{2,1,0:T(8,128)S(1)}) custom-call(s32[2]{0:T(128)S(1)} %copy-done.28, bf16[8,128,512]{2,1,0:T(8,128)(2,1)S(1)} %bitcast.45, f32[8,1,512]{2,1,0:T(1,128)S(1)} %bitcast.70, bf16[32,512]{1,0:T(8,128)(2,1)S(1)} %bitcast.79, bf16[192,3072]{1,0:T(8,128)(2,1)S(1)} %copy-done.7), custom_call_target="tpu_custom_call" | custom-call | flops 52428800 | bytes 1048576 | tf_op jit(solution)/shard_map/small_sums/pallas_call | solution.py:147
  16.5 3.6 %project_other.4.refs_17_ = bf16[192,3072]{1,0:T(8,128)(2,1)} custom-call(s32[2]{0:T(128)S(1)} %copy-done.28, bf16[8,128,512]{2,1,0:T(8,128)(2,1)S(1)} %bitcast.46, bf16[8,128,512]{2,1,0:T(8,128)(2,1)S(1)} %bitcast.47, bf16[8,128,512]{2,1,0:T(8,128)(2,1)S(1)} %bitcast.48, bf16[8,128,512]{2,1,0:T(8,128)(2,1)S(1)} %bitcast.49, f32[8,1,512]{2,1,0:T(1,128)S(1)} %bitcast.71, ...), custom_call_target="tpu_custom_call" | custom-call | flops 603979776 | bytes 4325376 | tf_op jit(solution)/shard_map/project_other/pallas_call | solution.py:289
  20.3 2.9 %collective-permute-start.4 = (f32[4,16,128]{2,1,0:T(8,128)S(1)}, f32[4,16,128]{2,1,0:T(8,128)S(1)}, u32[]{:S(2)}, u32[]{:S(2)}) collective-permute-start(f32[4,16,128]{2,1,0:T(8,128)S(1)} %get-tuple-element.56), channel_id=1, source_target_pairs={{0,16},{4,20},{8,24},{12,28},{16,0},{20,4},{24,8},{28,12},{1,17},{... | collective-permute-start | bytes 98312 | tf_op jit(solution)/shard_map/ppermute | solution.py:525
  24.7 4.6 %project_own.1 = (f32[192,3072]{1,0:T(8,128)S(1)}, f32[192,3072]{1,0:T(8,128)S(1)}, f32[128,3072]{1,0:T(8,128)S(1)}) custom-call(s32[2]{0:T(128)S(1)} %copy-done.28, bf16[8,128,512]{2,1,0:T(8,128)(2,1)S(1)} %bitcast.53, bf16[8,128,512]{2,1,0:T(8,128)(2,1)S(1)} %bitcast.51, bf16[8,128,512]{2,1,0:T(8,128)(2,1)S(1)} %bitcast.52, ...), custom_call_target="tpu_custom_call" | custom-call | flops 1610612736 | bytes 6291456 | tf_op jit(solution)/shard_map/project_own/pallas_call | solution.py:289
  34.0 3.0 %collective-permute-done.other_ref = bf16[192,3072]{1,0:T(8,128)(2,1)S(1)} collective-permute-done((bf16[192,3072]{1,0:T(8,128)(2,1)}, bf16[192,3072]{1,0:T(8,128)(2,1)S(1)}, u32[]{:S(2)}, u32[]{:S(2)}) %collective-permute-start) | collective-permute-done | bytes 1179680 | tf_op jit(solution)/shard_map/ppermute | solution.py:525
  37.0 1.8 fold.6
  40.5 2.0 %collective-permute-start.1 = (bf16[96,3072]{1,0:T(8,128)(2,1)}, bf16[96,3072]{1,0:T(8,128)(2,1)}, u32[]{:S(2)}, u32[]{:S(2)}) collective-permute-start(bf16[96,3072]{1,0:T(8,128)(2,1)} %get-tuple-element.49), channel_id=1, source_target_pairs={{0,8},{4,12},{8,0},{12,4},{16,24},{20,28},{24,16},{28,20},{1,9},{5... | collective-permute-start | bytes 1769480 | tf_op jit(solution)/shard_map/ppermute | solution.py:525
  52.2 3.3 %project_other.5._ = bf16[128,3072]{1,0:T(8,128)(2,1)} custom-call(s32[2]{0:T(128)S(1)} %copy-done.29, bf16[8,128,512]{2,1,0:T(8,128)(2,1)S(1)} %bitcast.62, bf16[8,128,512]{2,1,0:T(8,128)(2,1)S(1)} %bitcast.63, bf16[8,128,512]{2,1,0:T(8,128)(2,1)S(1)} %bitcast.64, bf16[8,128,512]{2,1,0:T(8,128)(2,1)S(1)} %bitcast.65, f32[8,1,512]{2,1,0:T(1,128)S(1)} %bitcast.73, ...), custom_call_target="tpu_custom_call" | custom-call | flops 402653184 | bytes 3932160 | tf_op jit(solution)/shard_map/project_other/pallas_call | solution.py:289
  56.0 2.3 %fold.7 = (f32[48,3072]{1,0:T(8,128)S(1)}, bf16[48,3072]{1,0:T(8,128)(2,1)S(1)}, f32[8,128]{1,0:T(8,128)S(1)}) custom-call(f32[96,3072]{1,0:T(8,128)S(1)} %copy-done.14, bf16[96,3072]{1,0:T(8,128)(2,1)} %collective-permute-done.1.other_ref, bf16[128,3072]{1,0:T(8,128)(2,1)} %project_other.5._), custom_call_target="tpu_custom_call" | custom-call | flops 589824 | bytes 2654208 | tf_op jit(solution)/shard_map/fold/pallas_call | solution.py:319
  59.1 3.3 %collective-permute-done.3.other_ref = bf16[192,3072]{1,0:T(8,128)(2,1)} collective-permute-done((bf16[192,3072]{1,0:T(8,128)(2,1)}, bf16[192,3072]{1,0:T(8,128)(2,1)}, u32[]{:S(2)}, u32[]{:S(2)}) %collective-permute-start.3) | collective-permute-done | bytes 1179680 | tf_op jit(solution)/shard_map/ppermute | solution.py:525
  62.4 2.3 %fold.8 = (f32[96,3072]{1,0:T(8,128)S(1)}, bf16[96,3072]{1,0:T(8,128)(2,1)S(1)}, f32[8,128]{1,0:T(8,128)S(1)}) custom-call(f32[192,3072]{1,0:T(8,128)S(1)} %copy-done.10, bf16[192,3072]{1,0:T(8,128)(2,1)} %collective-permute-done.3.other_ref, f32[8,128]{1,0:T(8,128)S(1)} %get-tuple-element.54._), custom_call_target="tpu_custom_call" | custom-call | flops 1179648 | bytes 5308416 | tf_op jit(solution)/shard_map/fold/pallas_call | solution.py:319
  71.3 3.0 %collective-permute-start.2 = (bf16[48,3072]{1,0:T(8,128)(2,1)}, bf16[48,3072]{1,0:T(8,128)(2,1)S(1)}, u32[]{:S(2)}, u32[]{:S(2)}) collective-permute-start(bf16[48,3072]{1,0:T(8,128)(2,1)} %copy-done.42), channel_id=1, source_target_pairs={{0,16},{4,20},{8,24},{12,28},{16,0},{20,4},{24,8},{28,12},{1,17},{... | collective-permute-start | bytes 884744 | tf_op jit(solution)/shard_map/ppermute | solution.py:525
  84.9 11.1 %collective-permute-done.7.other_ref = bf16[96,3072]{1,0:T(8,128)(2,1)} collective-permute-done((bf16[96,3072]{1,0:T(8,128)(2,1)}, bf16[96,3072]{1,0:T(8,128)(2,1)}, u32[]{:S(2)}, u32[]{:S(2)}) %collective-permute-start.7) | collective-permute-done | bytes 589856 | tf_op jit(solution)/shard_map/ppermute | solution.py:525
  97.2 3.2 %fold.10 = (f32[48,3072]{1,0:T(8,128)S(1)}, bf16[48,3072]{1,0:T(8,128)(2,1)}, f32[8,128]{1,0:T(8,128)S(1)}) custom-call(f32[96,3072]{1,0:T(8,128)S(1)} %copy-done.16, bf16[96,3072]{1,0:T(8,128)(2,1)} %collective-permute-done.7.other_ref, f32[8,128]{1,0:T(8,128)S(1)} %get-tuple-element.60._), custom_call_target="tpu_custom_call" | custom-call | flops 589824 | bytes 2654208 | tf_op jit(solution)/shard_map/fold/pallas_call | solution.py:319
  101.6 2.1 %path_weights.1 = (f32[4,128,128]{2,1,0:T(8,128)S(1)}, f32[4,128,4]{2,1,0:T(8,128)S(1)}) custom-call(s32[2]{0:T(128)S(1)} %copy-done.30, f32[16,128]{1,0:T(8,128)S(1)} %copy-done.33, f32[16,128]{1,0:T(8,128)} %collective-permute-done.6.far_ref, f32[16]{0:T(128)S(1)} %copy-done.40, s32[128,1]{1,0:T(8,128)S(1)} %copy-done.27, f32[128,4]{1,0:T(8,128)S(1)} %bitcast.74, ...), custom_call_target="tpu_custom_call" | custom-call | flops 1310720 | bytes 262144 | tf_op jit(solution)/shard_map/path_weights/pallas_call | solution.py:209
  104.9 4.7 %tree_read.3 = (bf16[48,1024]{1,0:T(8,128)(2,1)S(1)}, f32[8,128]{1,0:T(8,128)S(1)}) custom-call(f32[48,3072]{1,0:T(8,128)S(1)} %copy-done.20, bf16[48,3072]{1,0:T(8,128)(2,1)S(1)} %collective-permute-done.2.refs_0_, f32[32,4,128,256]{3,2,1,0:T(8,128)} %mat_ref.7, f32[4,32,128]{2,1,0:T(8,128)S(1)} %bitcast.66, f32[4,48,48]{2,1,0:T(8,128)S(1)} %get-tuple-element.107.refs_3_, ...), custom_call_target="tpu_custom_call" | custom-call | flops 603979776 | bytes 6291456 | tf_op jit(solution)/shard_map/tree_read/pallas_call | solution.py:398
  109.6 1.9 %collective-permute-start.9 = (bf16[48,1024]{1,0:T(8,128)(2,1)S(1)}, bf16[48,1024]{1,0:T(8,128)(2,1)S(1)}, u32[]{:S(2)}, u32[]{:S(2)}) collective-permute-start(bf16[48,1024]{1,0:T(8,128)(2,1)S(1)} %get-tuple-element.64.refs_0_), channel_id=1, source_target_pairs={{0,16},{4,20},{8,24},{12,28},{16,0},{20,4},{24,8},{28,12},{1,17},{... | collective-permute-start | bytes 294920 | tf_op jit(solution)/shard_map/ppermute | solution.py:525
  113.5 4.2 %commit_matrix.4 = (f32[32,4,128,256]{3,2,1,0:T(8,128)}, f32[8,128]{1,0:T(8,128)}) custom-call(f32[32,4,128,256]{3,2,1,0:T(8,128)} %mat_ref.7, bf16[32,16,512]{2,1,0:T(8,128)(2,1)} %maximum_maximum_fusion.1.left_ref, bf16[32,16,1024]{2,1,0:T(8,128)(2,1)} %maximum_maximum_fusion.right_ref, f32[32,1,4]{2,1,0:T(1,128)} %copy.45.decay_ref, f32[8,128]{1,0:T(8,128)} %copy-done.39), custom_call_target="tpu_custom_call" | custom-call | flops 536870912 | bytes 8388608 | tf_op jit(solution)/shard_map/commit_matrix/pallas_call | solution.py:91
  117.7 4.2 %commit_matrix.5 = (f32[32,4,128,256]{3,2,1,0:T(8,128)}, f32[8,128]{1,0:T(8,128)}) custom-call(f32[32,4,128,256]{3,2,1,0:T(8,128)} %mat_ref.7, bf16[32,16,512]{2,1,0:T(8,128)(2,1)} %maximum_maximum_fusion.1.left_ref, bf16[32,16,1024]{2,1,0:T(8,128)(2,1)} %maximum_maximum_fusion.right_ref, ...), custom_call_target="tpu_custom_call", output_to_operand_aliasing={{0}: (5, {})} | custom-call | flops 536870912 | bytes 8388608 | tf_op jit(solution)/shard_map/commit_matrix/pallas_call | solution.py:91
  124.0 4.7 %tree_read.4 = (bf16[48,1024]{1,0:T(8,128)(2,1)S(1)}, f32[8,128]{1,0:T(8,128)S(1)}) custom-call(f32[48,3072]{1,0:T(8,128)S(1)} %get-tuple-element.70.own_ref, bf16[48,3072]{1,0:T(8,128)(2,1)S(1)} %collective-permute-done.12.refs_0_, f32[32,4,128,256]{3,2,1,0:T(8,128)} %mat_ref.7, f32[4,32,128]{2,1,0:T(8,128)S(1)} %bitcast.67, ...), custom_call_target="tpu_custom_call" | custom-call | flops 603979776 | bytes 6291456 | tf_op jit(solution)/shard_map/tree_read/pallas_call | solution.py:398
  128.8 1.9 %collective-permute-start.14 = (bf16[48,1024]{1,0:T(8,128)(2,1)S(1)}, bf16[48,1024]{1,0:T(8,128)(2,1)S(1)}, u32[]{:S(2)}, u32[]{:S(2)}) collective-permute-start(bf16[48,1024]{1,0:T(8,128)(2,1)S(1)} %get-tuple-element.75.refs_4_), channel_id=1, source_target_pairs={{0,16},{4,20},{8,24},{12,28},{16,0},{20,4},{24,8},{28,12},{1,17},{... | collective-permute-start | bytes 294920 | tf_op jit(solution)/shard_map/ppermute | solution.py:525
  132.6 3.7 %tree_read.5 = (bf16[32,1024]{1,0:T(8,128)(2,1)S(1)}, f32[8,128]{1,0:T(8,128)S(1)}) custom-call(f32[32,3072]{1,0:T(8,128)S(1)} %get-tuple-element.76.own_ref, bf16[32,3072]{1,0:T(8,128)(2,1)S(1)} %collective-permute-done.15.refs_0_, f32[32,4,128,256]{3,2,1,0:T(8,128)} %mat_ref.7, f32[4,32,128]{2,1,0:T(8,128)S(1)} %bitcast.68, ...), custom_call_target="tpu_custom_call" | custom-call | flops 268435456 | bytes 4194304 | tf_op jit(solution)/shard_map/tree_read/pallas_call | solution.py:398
  141.2 4.2 %collective-permute-done.16.refs_6_ = bf16[96,1024]{1,0:T(8,128)(2,1)S(1)} collective-permute-done((bf16[96,1024]{1,0:T(8,128)(2,1)S(1)}, bf16[96,1024]{1,0:T(8,128)(2,1)S(1)}, u32[]{:S(2)}, u32[]{:S(2)}) %collective-permute-start.16) | collective-permute-done | bytes 196640 | tf_op jit(solution)/shard_map/ppermute | solution.py:525
  147.1 2.0 %collective-permute-start.20 = (bf16[32,1024]{1,0:T(8,128)(2,1)S(1)}, bf16[32,1024]{1,0:T(8,128)(2,1)S(1)}, u32[]{:S(2)}, u32[]{:S(2)}) collective-permute-start(bf16[32,1024]{1,0:T(8,128)(2,1)S(1)} %get-tuple-element.81.refs_0_), channel_id=1, source_target_pairs={{0,24},{4,28},{8,16},{12,20},{16,8},{20,12},{24,0},{28,4},{1,25},{... | collective-permute-start | bytes 196616 | tf_op jit(solution)/shard_map/ppermute | solution.py:525
  151.5 4.3 %commit_matrix.6 = (f32[32,4,128,256]{3,2,1,0:T(8,128)}, f32[8,128]{1,0:T(8,128)}) custom-call(f32[32,4,128,256]{3,2,1,0:T(8,128)} %mat_ref.7, bf16[32,16,512]{2,1,0:T(8,128)(2,1)} %maximum_maximum_fusion.1.left_ref, bf16[32,16,1024]{2,1,0:T(8,128)(2,1)} %maximum_maximum_fusion.right_ref, ...), custom_call_target="tpu_custom_call", output_to_operand_aliasing={{0}: (5, {})} | custom-call | flops 536870912 | bytes 8388608 | tf_op jit(solution)/shard_map/commit_matrix/pallas_call | solution.py:91
  159.0 4.1 %output_product.2 = (f32[2,2,96,512]{3,2,1,0:T(8,128)S(1)}, f32[2,2,96,512]{3,2,1,0:T(8,128)}) custom-call(s32[2]{0:T(128)S(1)} %copy-done.30, bf16[48,1024]{1,0:T(8,128)(2,1)S(1)} %get-tuple-element.64.refs_0_, bf16[48,1024]{1,0:T(8,128)(2,1)S(1)} %collective-permute-done.9.refs_1_, bf16[96,1024]{1,0:T(8,128)(2,1)S(1)} %collective-permute-done.11.refs_2_, ...), custom_call_target="tpu_custom_call" | custom-call | flops 805306368 | bytes 1048576 | tf_op jit(solution)/shard_map/output_product/pallas_call | solution.py:466
  164.1 7.7 %collective-permute-done.23.refs_4_ = bf16[128,1024]{1,0:T(8,128)(2,1)S(1)} collective-permute-done((bf16[128,1024]{1,0:T(8,128)(2,1)S(1)}, bf16[128,1024]{1,0:T(8,128)(2,1)S(1)}, u32[]{:S(2)}, u32[]{:S(2)}) %collective-permute-start.23) | collective-permute-done | bytes 262176 | tf_op jit(solution)/shard_map/ppermute | solution.py:525
  171.8 2.0 %output_product.3 = (f32[2,2,32,512]{3,2,1,0:T(8,128)S(1)}, f32[2,2,32,512]{3,2,1,0:T(8,128)S(1)}) custom-call(s32[2]{0:T(128)S(1)} %copy-done.30, bf16[32,1024]{1,0:T(8,128)(2,1)S(1)} %copy-done.25, bf16[32,1024]{1,0:T(8,128)(2,1)S(1)} %collective-permute-done.18.refs_1_, bf16[32,1024]{1,0:T(8,128)(2,1)S(1)} %collective-permute-done.19.refs_2_, ...), custom_call_target="tpu_custom_call" | custom-call | flops 268435456 | bytes 1048576 | tf_op jit(solution)/shard_map/output_product/pallas_call | solution.py:466
  177.9 4.2 %commit_matrix.7 = (f32[32,4,128,256]{3,2,1,0:T(8,128)}, f32[8,128]{1,0:T(8,128)}) custom-call(f32[32,4,128,256]{3,2,1,0:T(8,128)} %mat_ref.7, bf16[32,16,512]{2,1,0:T(8,128)(2,1)} %maximum_maximum_fusion.1.left_ref, bf16[32,16,1024]{2,1,0:T(8,128)(2,1)} %maximum_maximum_fusion.right_ref, ...), custom_call_target="tpu_custom_call", output_to_operand_aliasing={{0}: (5, {})} | custom-call | flops 536870912 | bytes 8388608 | tf_op jit(solution)/shard_map/commit_matrix/pallas_call | solution.py:91
  182.7 6.2 %collective-permute-done.22 = bf16[1,2,96,512]{3,2,1,0:T(8,128)(2,1)S(1)} collective-permute-done((bf16[1,2,96,512]{3,2,1,0:T(8,128)(2,1)S(1)}, bf16[1,2,96,512]{3,2,1,0:T(8,128)(2,1)S(1)}, u32[]{:S(2)}, u32[]{:S(2)}) %collective-permute-start.22) | collective-permute-done | bytes 196640 | tf_op jit(solution)/shard_map/ppermute | solution.py:525
  (216 shorter events, 67.3 us)
Async XLA Ops:
  6.9 30.1 %collective-permute-start = (bf16[192,3072]{1,0:T(8,128)(2,1)}, bf16[192,3072]{1,0:T(8,128)(2,1)S(1)}, u32[]{:S(2)}, u32[]{:S(2)}) collective-permute-start(bf16[192,3072]{1,0:T(8,128)(2,1)} %project_other.3._), channel_id=1, source_target_pairs={{0,4},{4,0},{8,12},{12,8},{16,20},{20,16},{24,28},{28,24},{1,5},{5... | collective-permute-start | bytes 3538952 | tf_op jit(solution)/shard_map/ppermute | solution.py:525
  20.1 42.3 %collective-permute-start.3 = (bf16[192,3072]{1,0:T(8,128)(2,1)}, bf16[192,3072]{1,0:T(8,128)(2,1)}, u32[]{:S(2)}, u32[]{:S(2)}) collective-permute-start(bf16[192,3072]{1,0:T(8,128)(2,1)} %project_other.4.refs_17_), channel_id=1, source_target_pairs={{0,4},{4,0},{8,12},{12,8},{16,20},{20,16},{24,28},{28,24},{1,5},{5... | collective-permute-start | bytes 3538952 | tf_op jit(solution)/shard_map/ppermute | solution.py:525
  20.3 11.5 %collective-permute-start.4 = (f32[4,16,128]{2,1,0:T(8,128)S(1)}, f32[4,16,128]{2,1,0:T(8,128)S(1)}, u32[]{:S(2)}, u32[]{:S(2)}) collective-permute-start(f32[4,16,128]{2,1,0:T(8,128)S(1)} %get-tuple-element.56), channel_id=1, source_target_pairs={{0,16},{4,20},{8,24},{12,28},{16,0},{20,4},{24,8},{28,12},{1,17},{... | collective-permute-start | bytes 98312 | tf_op jit(solution)/shard_map/ppermute | solution.py:525
  32.5 13.3 %collective-permute-start.5 = (f32[2,16,128]{2,1,0:T(8,128)}, f32[2,16,128]{2,1,0:T(8,128)}, u32[]{:S(2)}, u32[]{:S(2)}) collective-permute-start(f32[2,16,128]{2,1,0:T(8,128)} %slice.104), channel_id=1, source_target_pairs={{0,8},{4,12},{8,0},{12,4},{16,24},{20,28},{24,16},{28,20},{1,9},{5... | collective-permute-start | bytes 49160 | tf_op jit(solution)/shard_map/ppermute | solution.py:525
  40.5 15.5 %collective-permute-start.1 = (bf16[96,3072]{1,0:T(8,128)(2,1)}, bf16[96,3072]{1,0:T(8,128)(2,1)}, u32[]{:S(2)}, u32[]{:S(2)}) collective-permute-start(bf16[96,3072]{1,0:T(8,128)(2,1)} %get-tuple-element.49), channel_id=1, source_target_pairs={{0,8},{4,12},{8,0},{12,4},{16,24},{20,28},{24,16},{28,20},{1,9},{5... | collective-permute-start | bytes 1769480 | tf_op jit(solution)/shard_map/ppermute | solution.py:525
  47.2 54.3 %collective-permute-start.6 = (f32[16,128]{1,0:T(8,128)}, f32[16,128]{1,0:T(8,128)}, u32[]{:S(2)}, u32[]{:S(2)}) collective-permute-start(f32[16,128]{1,0:T(8,128)} %get-tuple-element.108), channel_id=1, source_target_pairs={{0,4},{4,0},{8,12},{12,8},{16,20},{20,16},{24,28},{28,24},{1,5},{5... | collective-permute-start | bytes 24584 | tf_op jit(solution)/shard_map/ppermute | solution.py:525
  55.5 23.5 %collective-permute-start.8 = (bf16[128,3072]{1,0:T(8,128)(2,1)}, bf16[128,3072]{1,0:T(8,128)(2,1)S(1)}, u32[]{:S(2)}, u32[]{:S(2)}) collective-permute-start(bf16[128,3072]{1,0:T(8,128)(2,1)} %project_other.5._), channel_id=1, source_target_pairs={{0,4},{4,0},{8,12},{12,8},{16,20},{20,16},{24,28},{28,24},{1,5},{5... | collective-permute-start | bytes 2359304 | tf_op jit(solution)/shard_map/ppermute | solution.py:525
  71.3 32.5 %collective-permute-start.2 = (bf16[48,3072]{1,0:T(8,128)(2,1)}, bf16[48,3072]{1,0:T(8,128)(2,1)S(1)}, u32[]{:S(2)}, u32[]{:S(2)}) collective-permute-start(bf16[48,3072]{1,0:T(8,128)(2,1)} %copy-done.42), channel_id=1, source_target_pairs={{0,16},{4,20},{8,24},{12,28},{16,0},{20,4},{24,8},{28,12},{1,17},{... | collective-permute-start | bytes 884744 | tf_op jit(solution)/shard_map/ppermute | solution.py:525
  74.3 21.7 %collective-permute-start.7 = (bf16[96,3072]{1,0:T(8,128)(2,1)}, bf16[96,3072]{1,0:T(8,128)(2,1)}, u32[]{:S(2)}, u32[]{:S(2)}) collective-permute-start(bf16[96,3072]{1,0:T(8,128)(2,1)} %copy-done.41), channel_id=1, source_target_pairs={{0,8},{4,12},{8,0},{12,4},{16,24},{20,28},{24,16},{28,20},{1,9},{5... | collective-permute-start | bytes 1769480 | tf_op jit(solution)/shard_map/ppermute | solution.py:525
  81.0 20.5 %copy-start.27 = (s32[128,1]{1,0:T(8,128)S(1)}, s32[128,1]{1,0:T(8,128)}, u32[]{:S(2)}) copy-start(s32[128,1]{1,0:T(8,128)} %reshape.85.parent_ref) | copy-start | bytes 1540
  81.0 20.5 %copy-start.30 = (s32[2]{0:T(128)S(1)}, s32[2]{0:T(128)}, u32[]{:S(2)}) copy-start(s32[2]{0:T(128)} %pad_add_fusion.pos_ref.refs_9_) | copy-start | bytes 28
  81.0 20.5 %copy-start.33 = (f32[16,128]{1,0:T(8,128)S(1)}, f32[16,128]{1,0:T(8,128)}, u32[]{:S(2)}) copy-start(f32[16,128]{1,0:T(8,128)} %get-tuple-element.109.near_ref) | copy-start | bytes 24580
  81.0 20.5 %copy-start.40 = (f32[16]{0:T(128)S(1)}, f32[16]{0:T(128)}, u32[]{:S(2)}) copy-start(f32[16]{0:T(128)} %bias_ref.1) | copy-start | bytes 196
  81.0 22.8 %copy-start.31 = (f32[1024]{0:T(1024)S(1)}, f32[1024]{0:T(1024)}, u32[]{:S(2)}) copy-start(f32[1024]{0:T(1024)} %param.27) | copy-start | bytes 12292
  82.7 28.9 %collective-permute-start.10 = (bf16[64,3072]{1,0:T(8,128)(2,1)}, bf16[64,3072]{1,0:T(8,128)(2,1)S(1)}, u32[]{:S(2)}, u32[]{:S(2)}) collective-permute-start(bf16[64,3072]{1,0:T(8,128)(2,1)} %get-tuple-element.66), channel_id=1, source_target_pairs={{0,8},{4,12},{8,0},{12,4},{16,24},{20,28},{24,16},{28,20},{1,9},{5... | collective-permute-start | bytes 1179656 | tf_op jit(solution)/shard_map/ppermute | solution.py:525
  100.4 22.9 %collective-permute-start.12 = (bf16[48,3072]{1,0:T(8,128)(2,1)}, bf16[48,3072]{1,0:T(8,128)(2,1)S(1)}, u32[]{:S(2)}, u32[]{:S(2)}) collective-permute-start(bf16[48,3072]{1,0:T(8,128)(2,1)} %get-tuple-element.71), channel_id=1, source_target_pairs={{0,16},{4,20},{8,24},{12,28},{16,0},{20,4},{24,8},{28,12},{1,17},{... | collective-permute-start | bytes 884744 | tf_op jit(solution)/shard_map/ppermute | solution.py:525
  109.6 21.1 %collective-permute-start.9 = (bf16[48,1024]{1,0:T(8,128)(2,1)S(1)}, bf16[48,1024]{1,0:T(8,128)(2,1)S(1)}, u32[]{:S(2)}, u32[]{:S(2)}) collective-permute-start(bf16[48,1024]{1,0:T(8,128)(2,1)S(1)} %get-tuple-element.64.refs_0_), channel_id=1, source_target_pairs={{0,16},{4,20},{8,24},{12,28},{16,0},{20,4},{24,8},{28,12},{1,17},{... | collective-permute-start | bytes 294920 | tf_op jit(solution)/shard_map/ppermute | solution.py:525
  112.5 20.2 %collective-permute-start.15 = (bf16[32,3072]{1,0:T(8,128)(2,1)S(1)}, bf16[32,3072]{1,0:T(8,128)(2,1)S(1)}, u32[]{:S(2)}, u32[]{:S(2)}) collective-permute-start(bf16[32,3072]{1,0:T(8,128)(2,1)S(1)} %get-tuple-element.77), channel_id=1, source_target_pairs={{0,16},{4,20},{8,24},{12,28},{16,0},{20,4},{24,8},{28,12},{1,17},{... | collective-permute-start | bytes 589832 | tf_op jit(solution)/shard_map/ppermute | solution.py:525
  128.8 8.1 %collective-permute-start.14 = (bf16[48,1024]{1,0:T(8,128)(2,1)S(1)}, bf16[48,1024]{1,0:T(8,128)(2,1)S(1)}, u32[]{:S(2)}, u32[]{:S(2)}) collective-permute-start(bf16[48,1024]{1,0:T(8,128)(2,1)S(1)} %get-tuple-element.75.refs_4_), channel_id=1, source_target_pairs={{0,16},{4,20},{8,24},{12,28},{16,0},{20,4},{24,8},{28,12},{1,17},{... | collective-permute-start | bytes 294920 | tf_op jit(solution)/shard_map/ppermute | solution.py:525
  131.4 7.6 %collective-permute-start.11 = (bf16[96,1024]{1,0:T(8,128)(2,1)S(1)}, bf16[96,1024]{1,0:T(8,128)(2,1)S(1)}, u32[]{:S(2)}, u32[]{:S(2)}) collective-permute-start(bf16[96,1024]{1,0:T(8,128)(2,1)S(1)} %maximum_add_fusion.3), channel_id=1, source_target_pairs={{0,8},{4,12},{8,0},{12,4},{16,24},{20,28},{24,16},{28,20},{1,9},{5... | collective-permute-start | bytes 589832 | tf_op jit(solution)/shard_map/ppermute | solution.py:525
  136.3 19.5 %copy-start.24 = (bf16[32,1024]{1,0:T(8,128)(2,1)}, bf16[32,1024]{1,0:T(8,128)(2,1)S(1)}, u32[]{:S(2)}) copy-start(bf16[32,1024]{1,0:T(8,128)(2,1)S(1)} %get-tuple-element.81.refs_0_) | copy-start | bytes 196612
  137.6 7.8 %collective-permute-start.16 = (bf16[96,1024]{1,0:T(8,128)(2,1)S(1)}, bf16[96,1024]{1,0:T(8,128)(2,1)S(1)}, u32[]{:S(2)}, u32[]{:S(2)}) collective-permute-start(bf16[96,1024]{1,0:T(8,128)(2,1)S(1)} %maximum_add_fusion.4), channel_id=1, source_target_pairs={{0,8},{4,12},{8,0},{12,4},{16,24},{20,28},{24,16},{28,20},{1,9},{5... | collective-permute-start | bytes 589832 | tf_op jit(solution)/shard_map/ppermute | solution.py:525
  139.7 16.8 %collective-permute-start.13 = (bf16[192,1024]{1,0:T(8,128)(2,1)S(1)}, bf16[192,1024]{1,0:T(8,128)(2,1)S(1)}, u32[]{:S(2)}, u32[]{:S(2)}) collective-permute-start(bf16[192,1024]{1,0:T(8,128)(2,1)S(1)} %maximum_add_fusion.refs_10_.refs_7_), channel_id=1, source_target_pairs={{0,4},{4,0},{8,12},{12,8},{16,20},{20,16},{24,28},{28,24},{1,5},{5... | collective-permute-start | bytes 1179656 | tf_op jit(solution)/shard_map/ppermute | solution.py:525
  146.1 10.4 %collective-permute-start.17 = (bf16[192,1024]{1,0:T(8,128)(2,1)S(1)}, bf16[192,1024]{1,0:T(8,128)(2,1)S(1)}, u32[]{:S(2)}, u32[]{:S(2)}) collective-permute-start(bf16[192,1024]{1,0:T(8,128)(2,1)S(1)} %maximum_add_fusion.1.refs_11_.refs_8_), channel_id=1, source_target_pairs={{0,4},{4,0},{8,12},{12,8},{16,20},{20,16},{24,28},{28,24},{1,5},{5... | collective-permute-start | bytes 1179656 | tf_op jit(solution)/shard_map/ppermute | solution.py:525
  147.1 8.7 %collective-permute-start.20 = (bf16[32,1024]{1,0:T(8,128)(2,1)S(1)}, bf16[32,1024]{1,0:T(8,128)(2,1)S(1)}, u32[]{:S(2)}, u32[]{:S(2)}) collective-permute-start(bf16[32,1024]{1,0:T(8,128)(2,1)S(1)} %get-tuple-element.81.refs_0_), channel_id=1, source_target_pairs={{0,24},{4,28},{8,16},{12,20},{16,8},{20,12},{24,0},{28,4},{1,25},{... | collective-permute-start | bytes 196616 | tf_op jit(solution)/shard_map/ppermute | solution.py:525
  149.1 6.7 %collective-permute-start.19 = (bf16[32,1024]{1,0:T(8,128)(2,1)S(1)}, bf16[32,1024]{1,0:T(8,128)(2,1)S(1)}, u32[]{:S(2)}, u32[]{:S(2)}) collective-permute-start(bf16[32,1024]{1,0:T(8,128)(2,1)S(1)} %get-tuple-element.81.refs_0_), channel_id=1, source_target_pairs={{0,8},{4,12},{8,0},{12,4},{16,24},{20,28},{24,16},{28,20},{1,9},{5... | collective-permute-start | bytes 196616 | tf_op jit(solution)/shard_map/ppermute | solution.py:525
  150.0 5.9 %collective-permute-start.18 = (bf16[32,1024]{1,0:T(8,128)(2,1)S(1)}, bf16[32,1024]{1,0:T(8,128)(2,1)S(1)}, u32[]{:S(2)}, u32[]{:S(2)}) collective-permute-start(bf16[32,1024]{1,0:T(8,128)(2,1)S(1)} %get-tuple-element.81.refs_0_), channel_id=1, source_target_pairs={{0,16},{4,20},{8,24},{12,28},{16,0},{20,4},{24,8},{28,12},{1,17},{... | collective-permute-start | bytes 196616 | tf_op jit(solution)/shard_map/ppermute | solution.py:525
  163.1 19.0 %collective-permute-start.21 = (f32[2,2,96,512]{3,2,1,0:T(8,128)}, f32[2,2,96,512]{3,2,1,0:T(8,128)S(1)}, u32[]{:S(2)}, u32[]{:S(2)}) collective-permute-start(f32[2,2,96,512]{3,2,1,0:T(8,128)} %get-tuple-element.83), channel_id=1, source_target_pairs={{0,1},{1,0},{2,3},{3,2},{4,5},{5,4},{6,7},{7,6},{8,9},{9,8},{10,11... | collective-permute-start | bytes 2359304 | tf_op jit(solution)/shard_map/ppermute | solution.py:525
  163.1 8.7 %collective-permute-start.23 = (bf16[128,1024]{1,0:T(8,128)(2,1)S(1)}, bf16[128,1024]{1,0:T(8,128)(2,1)S(1)}, u32[]{:S(2)}, u32[]{:S(2)}) collective-permute-start(bf16[128,1024]{1,0:T(8,128)(2,1)S(1)} %maximum_add_fusion.2.refs_12_.refs_9_), channel_id=1, source_target_pairs={{0,4},{4,0},{8,12},{12,8},{16,20},{20,16},{24,28},{28,24},{1,5},{5... | collective-permute-start | bytes 786440 | tf_op jit(solution)/shard_map/ppermute | solution.py:525
  173.9 1.6 collective-permute-start.24
  175.5 7.2 %collective-permute-start.25 = (bf16[1,2,32,512]{3,2,1,0:T(8,128)(2,1)S(1)}, bf16[1,2,32,512]{3,2,1,0:T(8,128)(2,1)S(1)}, u32[]{:S(2)}, u32[]{:S(2)}) collective-permute-start(bf16[1,2,32,512]{3,2,1,0:T(8,128)(2,1)S(1)} %slice.131.refs_0_), channel_id=1, source_target_pairs={{0,2},{1,3},{2,0},{3,1},{4,6},{5,7},{6,4},{7,5},{8,10},{9,11},{10,... | collective-permute-start | bytes 196616 | tf_op jit(solution)/shard_map/ppermute | solution.py:525
  182.2 6.7 %collective-permute-start.22 = (bf16[1,2,96,512]{3,2,1,0:T(8,128)(2,1)S(1)}, bf16[1,2,96,512]{3,2,1,0:T(8,128)(2,1)S(1)}, u32[]{:S(2)}, u32[]{:S(2)}) collective-permute-start(bf16[1,2,96,512]{3,2,1,0:T(8,128)(2,1)S(1)} %slice.130), channel_id=1, source_target_pairs={{0,2},{1,3},{2,0},{3,1},{4,6},{5,7},{6,4},{7,5},{8,10},{9,11},{10,... | collective-permute-start | bytes 589832 | tf_op jit(solution)/shard_map/ppermute | solution.py:525
  (52 other events, 273.2 us)
